TPU v7x, 256 devices: a whole 4x4x8 slice. The times are simulated.
256 devices in a mesh: fs: 32 (over z, x), tp: 8 (over y, core).
Axes of the slice: x: 4, y: 4, z: 8, core: 2. Of those that a mesh axis runs over, the one named last changes fastest.
Arguments:
- tokens: bfloat16 [6144, 2048], P('fs'), may hold values from -6 to 6
- norm_gain: float32 [2048], P('fs'), may hold values from 0.1 to 1.9
- expert_gate: float32 [64, 2048, 1024], P(None, 'fs', 'tp'), may hold values from -0.125 to 0.125
- expert_up: float32 [64, 2048, 1024], P(None, 'fs', 'tp'), may hold values from -0.125 to 0.125
- expert_down: float32 [64, 1024, 2048], P(None, 'fs', 'tp'), may hold values from -0.1875 to 0.1875
- shared_gate: float32 [2048, 1024], P('fs', 'tp'), may hold values from -0.125 to 0.125
- shared_up: float32 [2048, 1024], P('fs', 'tp'), may hold values from -0.125 to 0.125
- shared_down: float32 [1024, 2048], P('fs', 'tp'), may hold values from -0.1875 to 0.1875
- expert_ids: int32 [6144, 8], P('fs'), may hold values from 0 to 63, all different within a row; in each aligned block of 192 rows (0 to 191, 192 to 383, ...) at most 48 rows name the same one
- route_weights: float32 [6144, 8], P('fs'), may hold values from 0.25 to 1
Outputs:
- gate_ready: bfloat16 [64, 2048, 1024], P('fs', None, 'tp')
- up_ready: bfloat16 [64, 2048, 1024], P('fs', None, 'tp')
- down_ready: bfloat16 [64, 1024, 2048], P('fs', None, 'tp')
- shared_gate_ready: bfloat16 [2048, 1024], P(None, 'tp')
- shared_up_ready: bfloat16 [2048, 1024], P(None, 'tp')
- shared_down_ready: bfloat16 [1024, 2048], P(None, 'tp')
- mixed: bfloat16 [6144, 2048], P('fs', 'tp')
Inputs may be any that keep to these rules, and one draw needn't show every extreme that they name: `expert_ids`: each row names 8 different experts. Among the 192 rows of one index of fs no expert is named more than 48 times, and in every draw some expert is named exactly 48 times there.
All inputs are finite; a program needn't handle non-finite values.
Results may differ from a plain program's by a relative error of at most 0.0085.
Values may be sent and summed in bfloat16 or wider, within the bound.
A program may use at most 128 MiB of HBM per device.

v0:
```python
import jax
import jax.numpy as jnp
from jax import lax
from jax.sharding import PartitionSpec as P

TOP_K = 8
EPS = 1e-06


def cut_along(shard, dim, size):
    before, after = (shard.shape[:dim], shard.shape[dim + 1 :])
    return jnp.moveaxis(shard.reshape(*before, size, -1, *after), dim, 0)


def piece_ends(length, count):
    turn = length // count
    if turn >= 8:
        turn -= turn % 8
    return [turn * k for k in range(1, count)]


def in_order(parts, dim):
    parts = jnp.moveaxis(parts, 0, dim)
    shape = parts.shape
    return parts.reshape(*shape[:dim], shape[dim] * shape[dim + 1], *shape[dim + 2 :])


def several_exchanges(shard, axis, pieces, split_dim, concat_dim):
    parts = cut_along(shard, split_dim, lax.axis_size(axis))
    split_at = max(range(1, max(2, parts.ndim - 1)), key=lambda d: parts.shape[d])
    done = []
    for share in jnp.split(parts, piece_ends(parts.shape[split_at], pieces), axis=split_at):
        if share.size:
            done.append(lax.all_to_all(share, axis, split_axis=0, concat_axis=0, tiled=True))
    return in_order(jnp.concatenate(done, axis=split_at), concat_dim)


def side_by_side(arrays, axis, dim, along):
    ends, at = ([], 0)
    for a in arrays[:-1]:
        at += a.shape[along]
        ends.append(at)
    both = jnp.concatenate(arrays, axis=along)
    return tuple(jnp.split(lax.all_gather(both, axis, axis=dim, tiled=True), ends, axis=along))


def turned_gather(arrays, axis, dims):
    turned = [jnp.moveaxis(a, dim, 0) for a, dim in zip(arrays, dims)]
    widths = [t[0].size for t in turned]
    both = jnp.concatenate([t.reshape(-1, w) for t, w in zip(turned, widths)], axis=1)
    result = lax.all_gather(both, axis, axis=0, tiled=True)
    parts = jnp.split(result, [sum(widths[:k]) for k in range(1, len(widths))], axis=1)
    return tuple(
        (
            jnp.moveaxis(b.reshape(-1, *t.shape[1:]), 0, dim)
            for b, t, dim in zip(parts, turned, dims)
        )
    )


def expert_hidden(rows, gate_new, up_new):
    first = jnp.einsum("secn,enf->secf", rows, gate_new, preferred_element_type=jnp.float32)
    second = jnp.einsum("secn,enf->secf", rows, up_new, preferred_element_type=jnp.float32)
    return (jax.nn.silu(first) * second).astype(jnp.bfloat16)


def body(
    tokens,
    norm_gain,
    expert_gate,
    expert_up,
    expert_down,
    shared_gate,
    shared_up,
    shared_down,
    expert_ids,
    route_weights,
):
    groups = lax.axis_size("fs")
    experts = expert_gate.shape[0]
    per_group = experts // groups
    tok_count = tokens.shape[0]
    capacity = 2 * tok_count * TOP_K // experts
    gate_local = (expert_gate * norm_gain[None, :, None]).astype(jnp.bfloat16)
    up_local = (expert_up * norm_gain[None, :, None]).astype(jnp.bfloat16)
    down_local = expert_down.astype(jnp.bfloat16)
    gate_local = gate_local.reshape((groups, per_group) + gate_local.shape[1:])
    up_local = up_local.reshape((groups, per_group) + up_local.shape[1:])
    down_local = down_local.reshape((groups, per_group) + down_local.shape[1:])
    shared_first_local = (shared_gate * norm_gain[:, None]).astype(jnp.bfloat16)
    shared_second_local = (shared_up * norm_gain[:, None]).astype(jnp.bfloat16)
    shared_third_local = shared_down.astype(jnp.bfloat16)
    gate_moved, up_moved = (
        several_exchanges(gate_local, "fs", 2, 0, 2),
        several_exchanges(up_local, "fs", 2, 0, 2),
    )
    gate_ready = gate_moved[0]
    up_ready = up_moved[0]
    shared_gate_ready, shared_up_ready, shared_down_ready = (
        *side_by_side((shared_first_local, shared_second_local), "fs", 0, 1),
        lax.all_gather(shared_third_local, "fs", axis=0, tiled=True),
    )
    wide = tokens.astype(jnp.float32)
    normed = (wide * lax.rsqrt(jnp.mean(wide * wide, axis=-1, keepdims=True) + EPS)).astype(
        jnp.bfloat16
    )
    chosen = expert_ids.reshape(-1)
    onehot = (chosen[:, None] == jnp.arange(experts, dtype=jnp.int32)[None, :]).astype(jnp.int32)
    ranks = jnp.sum(jnp.cumsum(onehot, axis=0) * onehot, axis=1) - 1
    owners = jnp.arange(tok_count * TOP_K, dtype=jnp.int32) // TOP_K
    slot_token = jnp.zeros((experts, capacity), jnp.int32).at[chosen, ranks].set(owners)
    outgoing = normed[slot_token.reshape(-1)].reshape(groups, per_group, capacity, normed.shape[1])
    share = capacity // lax.axis_size("tp")
    mine = lax.dynamic_slice_in_dim(outgoing, lax.axis_index("tp") * share, share, 2)
    arrived = lax.all_to_all(mine, "fs", split_axis=0, concat_axis=0, tiled=True)
    hidden = expert_hidden(lax.all_gather(arrived, "tp", axis=2, tiled=True), gate_ready, up_ready)
    shared_first = jnp.dot(normed, shared_gate_ready, preferred_element_type=jnp.float32)
    shared_second = jnp.dot(normed, shared_up_ready, preferred_element_type=jnp.float32)
    shared_hidden = (jax.nn.silu(shared_first) * shared_second).astype(jnp.bfloat16)[None, None]
    down_moved = lax.all_to_all(down_local, "fs", split_axis=0, concat_axis=2, tiled=True)
    down_ready = down_moved[0]
    columns = down_ready.shape[2]
    routed_piece, shared_piece = turned_gather((hidden, shared_hidden), "tp", (3, 3))
    routed_total = jnp.einsum(
        "secf,efd->secd", routed_piece, down_ready, preferred_element_type=jnp.float32
    )
    shared_total = jnp.einsum(
        "abtf,fd->abtd", shared_piece, shared_down_ready, preferred_element_type=jnp.float32
    )
    returned = lax.all_to_all(
        routed_total.astype(jnp.bfloat16), "fs", split_axis=0, concat_axis=0, tiled=True
    )
    returned = returned.reshape(experts * capacity, columns)
    picked = (
        returned[chosen * capacity + ranks].astype(jnp.float32).reshape(tok_count, TOP_K, columns)
    )
    routed = jnp.sum(picked * route_weights[:, :, None], axis=1)
    mixed = (shared_total[0, 0] + routed).astype(jnp.bfloat16)
    return (
        gate_ready,
        up_ready,
        down_ready,
        shared_gate_ready,
        shared_up_ready,
        shared_down_ready,
        mixed,
    )


def solution(mesh):
    in_specs = (
        P("fs", None),
        P("fs"),
        P(None, "fs", "tp"),
        P(None, "fs", "tp"),
        P(None, "fs", "tp"),
        P("fs", "tp"),
        P("fs", "tp"),
        P("fs", "tp"),
        P("fs", None),
        P("fs", None),
    )
    out_specs = (
        P("fs", None, "tp"),
        P("fs", None, "tp"),
        P("fs", None, "tp"),
        P(None, "tp"),
        P(None, "tp"),
        P(None, "tp"),
        P("fs", "tp"),
    )
    return jax.shard_map(body, mesh=mesh, in_specs=in_specs, out_specs=out_specs, check_vma=False)
```

profile of v0, /device:TPU:32, one launch (start us, length us, event | category | flops | bytes accessed | tf_op | source)
XLA Modules:
  0.0 414.8 jit_solution(16375426263147226016)
XLA Ops:
  8.4 18.1 %reduce-window.6 = s32[64,12,128]{2,1,0:T(8,128)S(1)} reduce-window(s32[64,12,128]{2,1,0:T(8,128)S(1)} %fusion.25, s32[]{:T(128)} %constant.44.clone.1), window={size=1x1x128 pad=0_0x0_0x127_0}, to_apply=%region_1.0 | reduce-window | flops 12484608 | bytes 786436 | tf_op jit(solution)/shard_map/reduce-window
  27.8 6.2 %scatter_custom_fusion = s32[3072]{0:T(1024)S(1)} fusion(s32[1536]{0:T(1024)S(1)} %get-tuple-element.23, s32[1536]{0:T(1024)S(1)} %get-tuple-element.22, s32[]{:T(128)} %constant.44.clone.1), kind=kCustom, calls=%fused_computation.63 | custom fusion | bytes 12292
  34.7 15.9 %gather_fusion = bf16[3072,2048]{1,0:T(8,128)(2,1)} fusion(bf16[192,2048]{1,0:T(8,128)(2,1)S(1)} %fusion.11, s32[3072]{0:T(1024)S(1)} %broadcast_clamp_fusion), kind=kCustom, calls=%fused_computation | custom fusion | bytes 25178112 | tf_op jit(solution)/shard_map/gather | solution.py:112
  50.7 3.0 constant_dynamic-slice_fusion
  53.7 2.8 copy.64
  56.5 11.3 %all-to-all-start.5 = ((bf16[32,2,6,2048]{3,1,2,0:T(2,128)(2,1)}), bf16[32,2,6,2048]{3,1,2,0:T(2,128)(2,1)S(1)}, u32[]{:S(2)}, u32[]{:S(2)}) async-start(bf16[32,2,6,2048]{3,1,2,0:T(2,128)(2,1)} %copy.64), calls=%async_computation.5 | async-start | bytes 3145728 | tf_op jit(solution)/shard_map/all_to_all | solution.py:115
  68.6 38.4 %all-to-all-done.5 = bf16[32,2,6,2048]{3,1,2,0:T(2,128)(2,1)S(1)} async-done(((bf16[32,2,6,2048]{3,1,2,0:T(2,128)(2,1)}), bf16[32,2,6,2048]{3,1,2,0:T(2,128)(2,1)S(1)}, u32[]{:S(2)}, u32[]{:S(2)}) %all-to-all-start.5) | async-done | bytes 1572896 | tf_op jit(solution)/shard_map/all_to_all | solution.py:115
  107.1 2.0 copy.65
  109.1 2.8 multiply_convert_fusion
  112.9 23.9 %all_to_all.45 = bf16[32,1,2,32,128]{4,3,2,1,0:T(8,128)(2,1)S(1)} all-to-all(bf16[32,1,2,32,128]{4,3,2,1,0:T(8,128)(2,1)S(1)} %get-tuple-element.11), channel_id=1, replica_groups=mesh['fs'=32,'tp'=8] {'fs'}, dimensions={0} | all-to-all | bytes 1048576 | tf_op jit(solution)/shard_map/all_to_all | solution.py:34
  136.8 5.0 %all-to-all-start.1 = ((bf16[32,1,2,32,128]{4,3,2,1,0:T(8,128)(2,1)}), bf16[32,1,2,32,128]{4,3,2,1,0:T(8,128)(2,1)S(1)}, u32[]{:S(2)}, u32[]{:S(2)}) async-start(bf16[32,1,2,32,128]{4,3,2,1,0:T(8,128)(2,1)} %get-tuple-element.12), calls=%async_computation.1 | async-start | bytes 1048576 | tf_op jit(solution)/shard_map/all_to_all | solution.py:34
  142.8 15.6 %all-to-all-done.1 = bf16[32,1,2,32,128]{4,3,2,1,0:T(8,128)(2,1)S(1)} async-done(((bf16[32,1,2,32,128]{4,3,2,1,0:T(8,128)(2,1)}), bf16[32,1,2,32,128]{4,3,2,1,0:T(8,128)(2,1)S(1)}, u32[]{:S(2)}, u32[]{:S(2)}) %all-to-all-start.1) | async-done | bytes 524320 | tf_op jit(solution)/shard_map/all_to_all | solution.py:34
  158.4 21.5 %all_to_all.46 = bf16[32,1,2,32,128]{4,3,2,1,0:T(8,128)(2,1)S(1)} all-to-all(bf16[32,1,2,32,128]{4,3,2,1,0:T(8,128)(2,1)S(1)} %get-tuple-element.9), channel_id=1, replica_groups=mesh['fs'=32,'tp'=8] {'fs'}, dimensions={0} | all-to-all | bytes 1048576 | tf_op jit(solution)/shard_map/all_to_all | solution.py:34
  179.9 5.1 %all-to-all-start.3 = ((bf16[32,1,2,32,128]{4,3,2,1,0:T(8,128)(2,1)}), bf16[32,1,2,32,128]{4,3,2,1,0:T(8,128)(2,1)S(1)}, u32[]{:S(2)}, u32[]{:S(2)}) async-start(bf16[32,1,2,32,128]{4,3,2,1,0:T(8,128)(2,1)} %get-tuple-element.10), calls=%async_computation.3 | async-start | bytes 1048576 | tf_op jit(solution)/shard_map/all_to_all | solution.py:34
  185.5 16.0 %all-to-all-done.3 = bf16[32,1,2,32,128]{4,3,2,1,0:T(8,128)(2,1)S(1)} async-done(((bf16[32,1,2,32,128]{4,3,2,1,0:T(8,128)(2,1)}), bf16[32,1,2,32,128]{4,3,2,1,0:T(8,128)(2,1)S(1)}, u32[]{:S(2)}, u32[]{:S(2)}) %all-to-all-start.3) | async-done | bytes 524320 | tf_op jit(solution)/shard_map/all_to_all | solution.py:34
  204.5 18.0 %all-gather.6.cloned.1.call-done = bf16[32,2,48,2048]{3,0,1,2:T(8,128)(2,1)} async-done(((bf16[32,2,6,2048]{3,0,1,2:T(8,128)(2,1)}), bf16[32,2,48,2048]{3,0,1,2:T(8,128)(2,1)}) %all-gather.6.cloned.1.call-update) | async-done | bytes 12582928 | tf_op jit(solution)/shard_map/all_gather | solution.py:116
  222.5 18.0 %fusion.2 = f32[2,128,32,48]{1,3,2,0:T(8,128)S(1)} fusion(bf16[2,2048,128,1]{2,1,3,0:T(8,128)(2,1)S(1)} %bitcast.105, bf16[32,2,48,2048]{3,0,1,2:T(8,128)(2,1)} %all-gather.6.cloned.1.call-done), kind=kOutput, calls=%fused_computation.5 | convolution fusion | flops 1610612736 | bytes 15204352 | tf_op jit(solution)/shard_map/secn,enf->secf/dot_general | solution.py:62
  240.6 13.8 %fusion.13 = bf16[128,32,2,48]{0,3,1,2:T(8,128)(2,1)S(1)} fusion(f32[2,128,32,48]{1,3,2,0:T(8,128)S(1)} %fusion.2, bf16[2,2048,128,1]{2,1,3,0:T(8,128)(2,1)S(1)} %bitcast.107, bf16[32,2,48,2048]{3,0,1,2:T(8,128)(2,1)} %all-gather.6.cloned.1.call-done), kind=kOutput, calls=%fused_computation.20 | convolution fusion | flops 1612972032 | bytes 15990784 | tf_op jit(solution)/shard_map/secn,enf->secf/dot_general | solution.py:63
  256.4 37.4 %all_to_all.47 = bf16[32,2,32,256]{3,2,1,0:T(8,128)(2,1)S(1)} all-to-all(bf16[32,2,32,256]{3,2,1,0:T(8,128)(2,1)S(1)} %bitcast.101), channel_id=1, replica_groups=mesh['fs'=32,'tp'=8] {'fs'}, dimensions={0} | all-to-all | bytes 2097152 | tf_op jit(solution)/shard_map/all_to_all | solution.py:120
  293.9 10.6 %all-gather.8.cloned.1.call-done = bf16[1024,3264]{0,1:T(8,128)(2,1)} async-done(((bf16[128,3264]{0,1:T(8,128)(2,1)}), bf16[1024,3264]{0,1:T(8,128)(2,1)}) %all-gather.8.cloned.1.call-update) | async-done | bytes 6684688 | tf_op jit(solution)/shard_map/all_gather | solution.py:51
  304.6 2.8 slice-done
  310.6 10.2 %all-to-all-start.6 = ((bf16[32,2,48,256]{3,2,1,0:T(8,128)(2,1)}), bf16[32,2,48,256]{3,2,1,0:T(8,128)(2,1)S(1)}, u32[]{:S(2)}, u32[]{:S(2)}) async-start(bf16[32,2,48,256]{3,2,1,0:T(8,128)(2,1)} %copy.70), calls=%async_computation.6 | async-start | bytes 3145728 | tf_op jit(solution)/shard_map/all_to_all | solution.py:130
  320.9 79.3 %all_gather.13 = bf16[1024,256]{1,0:T(8,128)(2,1)S(1)} all-gather(bf16[32,256]{1,0:T(8,128)(2,1)S(1)} %convert_element_type.57), channel_id=1, replica_groups=mesh['fs'=32,'tp'=8] {'fs'}, dimensions={0}, use_global_device_ids=true | all-gather | bytes 540672 | tf_op jit(solution)/shard_map/all_gather | solution.py:101
  400.3 4.8 %gather_fusion.1 = bf16[1536,256]{1,0:T(8,128)(2,1)S(1)} fusion(bf16[3072,256]{1,0:T(8,128)(2,1)S(1)} %bitcast.96, s32[2048]{0:T(1024)S(1)} %pad_clamp_fusion), kind=kCustom, calls=%fused_computation.1 | custom fusion | bytes 1579008 | tf_op jit(solution)/shard_map/gather | solution.py:135
  (84 shorter events, 17.9 us)
Async XLA Ops:
  8.3 19.2 %copy-start.13 = (s32[2]{0:T(128)S(1)}, s32[2]{0:T(128)}, u32[]{:S(2)}) copy-start(s32[2]{0:T(128)} %constant.57) | copy-start | bytes 28
  8.4 19.3 %copy-start.12 = (s32[2]{0:T(128)S(1)}, s32[2]{0:T(128)}, u32[]{:S(2)}) copy-start(s32[2]{0:T(128)} %constant.60) | copy-start | bytes 28
  8.4 25.9 %copy-start = (bf16[192,2048]{1,0:T(8,128)(2,1)S(1)}, bf16[192,2048]{1,0:T(8,128)(2,1)}, u32[]{:S(2)}) copy-start(bf16[192,2048]{1,0:T(8,128)(2,1)} %param.10) | copy-start | bytes 2359300
  56.5 11.4 %copy-start.7 = (f32[64,128]{1,0:T(8,128)S(1)}, f32[64,128]{1,0:T(8,128)}, u32[]{:S(2)}) copy-start(f32[64,128]{1,0:T(8,128)} %param.15) | copy-start | bytes 98308
  56.5 11.4 %copy-start.8 = (f32[64,128]{1,0:T(8,128)S(1)}, f32[64,128]{1,0:T(8,128)}, u32[]{:S(2)}) copy-start(f32[64,128]{1,0:T(8,128)} %param.16) | copy-start | bytes 98308
  56.5 11.4 %copy-start.11 = (f32[64]{0:T(128)S(1)}, f32[64]{0:T(128)}, u32[]{:S(2)}) copy-start(f32[64]{0:T(128)} %param.11) | copy-start | bytes 772
  56.5 50.6 %all-to-all-start.5 = ((bf16[32,2,6,2048]{3,1,2,0:T(2,128)(2,1)}), bf16[32,2,6,2048]{3,1,2,0:T(2,128)(2,1)S(1)}, u32[]{:S(2)}, u32[]{:S(2)}) async-start(bf16[32,2,6,2048]{3,1,2,0:T(2,128)(2,1)} %copy.64), calls=%async_computation.5 | async-start | bytes 3145728 | tf_op jit(solution)/shard_map/all_to_all | solution.py:115
  67.8 133.9 %all-gather.4.cloned.1.call-start = ((), (), s32[]{:S(2)}) async-start(), calls=%async_computation.7 | async-start | bytes 1081344 | tf_op jit(solution)/shard_map/all_gather | solution.py:44
  68.6 153.9 %all-gather.6.cloned.1.call-start = ((), (), s32[]{:S(2)}) async-start(), calls=%async_computation.8 | async-start | bytes 14155776 | tf_op jit(solution)/shard_map/all_gather | solution.py:116
  136.8 21.6 %all-to-all-start.1 = ((bf16[32,1,2,32,128]{4,3,2,1,0:T(8,128)(2,1)}), bf16[32,1,2,32,128]{4,3,2,1,0:T(8,128)(2,1)S(1)}, u32[]{:S(2)}, u32[]{:S(2)}) async-start(bf16[32,1,2,32,128]{4,3,2,1,0:T(8,128)(2,1)} %get-tuple-element.12), calls=%async_computation.1 | async-start | bytes 1048576 | tf_op jit(solution)/shard_map/all_to_all | solution.py:34
  179.9 21.5 %all-to-all-start.3 = ((bf16[32,1,2,32,128]{4,3,2,1,0:T(8,128)(2,1)}), bf16[32,1,2,32,128]{4,3,2,1,0:T(8,128)(2,1)S(1)}, u32[]{:S(2)}, u32[]{:S(2)}) async-start(bf16[32,1,2,32,128]{4,3,2,1,0:T(8,128)(2,1)} %get-tuple-element.10), calls=%async_computation.3 | async-start | bytes 1048576 | tf_op jit(solution)/shard_map/all_to_all | solution.py:34
  185.0 119.6 %all-gather.8.cloned.1.call-start = ((), (), s32[]{:S(2)}) async-start(), calls=%async_computation.9 | async-start | bytes 7520256 | tf_op jit(solution)/shard_map/all_gather | solution.py:51
  185.4 37.0 %copy-start.3 = (bf16[1,2,32,64,128]{4,3,2,1,0:T(8,128)(2,1)}, bf16[1,2,32,64,128]{4,3,2,1,0:T(8,128)(2,1)S(1)}, u32[]{:S(2)}) copy-start(bf16[1,2,32,64,128]{4,3,2,1,0:T(8,128)(2,1)S(1)} %copy.55) | copy-start | bytes 3145732
  201.6 38.9 %copy-start.4 = (bf16[1,2,32,64,128]{4,3,2,1,0:T(8,128)(2,1)}, bf16[1,2,32,64,128]{4,3,2,1,0:T(8,128)(2,1)S(1)}, u32[]{:S(2)}) copy-start(bf16[1,2,32,64,128]{4,3,2,1,0:T(8,128)(2,1)S(1)} %copy.56) | copy-start | bytes 3145732
  203.3 0.8 copy-start.6
  203.3 37.2 %copy-start.2 = (bf16[2048,128]{1,0:T(8,128)(2,1)}, bf16[2048,128]{1,0:T(8,128)(2,1)S(1)}, u32[]{:S(2)}) copy-start(bf16[2048,128]{1,0:T(8,128)(2,1)S(1)} %get-tuple-element.34) | copy-start | bytes 1572868
  254.3 1.9 copy-start.1
  293.9 10.7 %copy-start.5 = (bf16[1,2,32,32,256]{4,3,2,1,0:T(8,128)(2,1)}, bf16[1,2,32,32,256]{4,3,2,1,0:T(8,128)(2,1)S(1)}, u32[]{:S(2)}) copy-start(bf16[1,2,32,32,256]{4,3,2,1,0:T(8,128)(2,1)S(1)} %copy.57) | copy-start | bytes 3145732
  304.6 2.8 slice-start
  310.6 10.2 %copy-start.10 = (f32[192,8]{0,1:T(8,128)S(1)}, f32[192,8]{0,1:T(8,128)}, u32[]{:S(2)}) copy-start(f32[192,8]{0,1:T(8,128)} %param.19) | copy-start | bytes 18436
  310.6 10.3 %copy-start.9 = (f32[32,256]{1,0:T(8,128)S(1)}, f32[32,256]{1,0:T(8,128)}, u32[]{:S(2)}) copy-start(f32[32,256]{1,0:T(8,128)} %param.17) | copy-start | bytes 98308
  310.6 89.7 %all-to-all-start.6 = ((bf16[32,2,48,256]{3,2,1,0:T(8,128)(2,1)}), bf16[32,2,48,256]{3,2,1,0:T(8,128)(2,1)S(1)}, u32[]{:S(2)}, u32[]{:S(2)}) async-start(bf16[32,2,48,256]{3,2,1,0:T(8,128)(2,1)} %copy.70), calls=%async_computation.6 | async-start | bytes 3145728 | tf_op jit(solution)/shard_map/all_to_all | solution.py:130
Sparse Core Ops, SparseCore 0:
  71.8 80.5 all-gather.3
  154.2 68.2 all-gather.5
  255.5 49.0 all-gather.7
where the time goes:
time: 416 us; the launch traced here: 415 us
  blocking collectives  162 us (39%)
  waiting for transfers between devices  98.7 us (24%)
  local copies, waits for them, and re-layouts  46.8 us (11%)
  matrix products  36.3 us (9%)
  starting transfers between devices  31.9 us (8%)
  other arithmetic  24.6 us (6%)
  between operations  14.2 us (3%)
    all_gather x1, blocking collectives, body(): lax.all_gather(shared_third_local, 'fs', axis=0, tiled=True)  79.3 us
    all_to_all x2, blocking collectives, several_exchanges(): lax.all_to_all(share, axis, split_axis=0, concat_axis=0, tiled=True)  45.4 us
    all_to_all x1, waiting for transfers between devices, body(): lax.all_to_all(mine, 'fs', split_axis=0, concat_axis=0, tiled=True)  38.4 us
    all_to_all x1, blocking collectives, body(): lax.all_to_all(down_local, 'fs', split_axis=0, concat_axis=2, tiled=True)  37.4 us
    all_to_all x2, waiting for transfers between devices, several_exchanges(): lax.all_to_all(share, axis, split_axis=0, concat_axis=0, tiled=True)  31.6 us
    another operation x3, other arithmetic  18.4 us
    dot_general x1, matrix products, expert_hidden(): jnp.einsum('secn,enf->secf', rows, gate_new, preferred_element_type=jnp.f...  18 us
    all_gather x1, waiting for transfers between devices, body(): lax.all_gather(arrived, 'tp', axis=2, tiled=True)  18 us
  transfers between devices with their start and end apart: 7, of which 5 were waited for; matrix products, arithmetic and copies ran while one was open for 3% of the time, Pallas kernels for 0%

commit v1 on v0

--- a/solution.py
+++ b/solution.py
@@ -96,9 +96,18 @@
     )
     gate_ready = gate_moved[0]
     up_ready = up_moved[0]
+
+    def mix_ticks_over_axis(u_in, k_dim):
+        store = []
+        axis_id = "fs"
+        for _ in range(lax.axis_size(axis_id)):
+            store.append(u_in)
+        lower = jnp.concatenate(store, axis=k_dim)
+        return lax.all_to_all(lower, axis_id, k_dim, k_dim, tiled=True)
+
     shared_gate_ready, shared_up_ready, shared_down_ready = (
         *side_by_side((shared_first_local, shared_second_local), "fs", 0, 1),
-        lax.all_gather(shared_third_local, "fs", axis=0, tiled=True),
+        mix_ticks_over_axis(shared_third_local, k_dim=0),
     )
     wide = tokens.astype(jnp.float32)
     normed = (wide * lax.rsqrt(jnp.mean(wide * wide, axis=-1, keepdims=True) + EPS)).astype(

time: 416 us -> 377 us (0.906)
  blocking collectives: 162 us -> 45.4 us
  waiting for transfers between devices: 98.7 us -> 144 us
  local copies, waits for them, and re-layouts: 46.8 us -> 65.7 us
  starting transfers between devices: 31.9 us -> 43.4 us
    all_gather x1 -> x0, blocking collectives: 79.3 us -> none  [body(): lax.all_gather(shared_third_local, 'fs', axis=0, tiled=True)]
    all_to_all x1 -> x0, blocking collectives: 37.4 us -> none  [body(): lax.all_to_all(down_local, 'fs', split_axis=0, concat_axis=2, tiled=True)]
    all_to_all x1, waiting for transfers between devices: 0.01 us -> 37.2 us  [body(): lax.all_to_all(routed_total.astype(jnp.bfloat16), 'fs', split_axis=0, con...]
    unnamed x33 -> x63, local copies, waits for them, and re-layouts: 9.3 us -> 27.5 us
    all_to_all x0 -> x2, starting transfers between devices: none -> 16.5 us  [the longest x1 10.1 us: body(): lax.all_to_all(down_local, 'fs', split_axis=0, concat_axis=2, tiled=True)]
    all_to_all x0 -> x2, waiting for transfers between devices: none -> 15.3 us  [the longest x1 8.16 us: body(): lax.all_to_all(down_local, 'fs', split_axis=0, concat_axis=2, tiled=True)]
    all_gather x1, waiting for transfers between devices: 10.6 us -> 3 us  [turned_gather(): result = lax.all_gather(both, axis, axis=0, tiled=True)]
    all_to_all x1, starting transfers between devices: 10.2 us -> 5.12 us  [body(): lax.all_to_all(routed_total.astype(jnp.bfloat16), 'fs', split_axis=0, con...]
  transfers between devices with their start and end apart: 7 -> 9, of which waited for: 5 -> 8; matrix products, arithmetic and copies ran while one was open for 3% -> 9% of each run, Pallas kernels for 0% -> 0%
where the time goes in v1:
time: 377 us; the launch traced here: 375 us
  waiting for transfers between devices  144 us (38%)
  local copies, waits for them, and re-layouts  65.7 us (17%)
  blocking collectives  45.4 us (12%)
  starting transfers between devices  43.4 us (12%)
  matrix products  36.3 us (10%)
  other arithmetic  26.2 us (7%)
  between operations  14.2 us (4%)
    all_to_all x2, blocking collectives, several_exchanges(): lax.all_to_all(share, axis, split_axis=0, concat_axis=0, tiled=True)  45.4 us
    all_to_all x1, waiting for transfers between devices, body(): lax.all_to_all(mine, 'fs', split_axis=0, concat_axis=0, tiled=True)  38.4 us
    all_to_all x1, waiting for transfers between devices, body(): lax.all_to_all(routed_total.astype(jnp.bfloat16), 'fs', split_axis=0, con...  37.2 us
    all_to_all x2, waiting for transfers between devices, several_exchanges(): lax.all_to_all(share, axis, split_axis=0, concat_axis=0, tiled=True)  31.6 us
    unnamed x63, local copies, waits for them, and re-layouts  27.5 us
    another operation x3, other arithmetic  18.4 us
    dot_general x1, matrix products, expert_hidden(): jnp.einsum('secn,enf->secf', rows, gate_new, preferred_element_type=jnp.f...  18 us
    all_gather x1, waiting for transfers between devices, body(): lax.all_gather(arrived, 'tp', axis=2, tiled=True)  18 us
  transfers between devices with their start and end apart: 9, of which 8 were waited for; matrix products, arithmetic and copies ran while one was open for 9% of the time, Pallas kernels for 0%

profile of v1, /device:TPU:32, one launch (start us, length us, event | category | flops | bytes accessed | tf_op | source)
XLA Modules:
  0.0 374.8 jit_solution(3604918386813535641)
XLA Ops:
  8.4 18.1 %reduce-window.6 = s32[64,12,128]{2,1,0:T(8,128)S(1)} reduce-window(s32[64,12,128]{2,1,0:T(8,128)S(1)} %fusion.25, s32[]{:T(128)} %constant.44.clone.1), window={size=1x1x128 pad=0_0x0_0x127_0}, to_apply=%region_1.0 | reduce-window | flops 12484608 | bytes 786436 | tf_op jit(solution)/shard_map/reduce-window
  27.8 6.2 %scatter_custom_fusion = s32[3072]{0:T(1024)S(1)} fusion(s32[1536]{0:T(1024)S(1)} %get-tuple-element.25, s32[1536]{0:T(1024)S(1)} %get-tuple-element.24, s32[]{:T(128)} %constant.44.clone.1), kind=kCustom, calls=%fused_computation.95 | custom fusion | bytes 12292
  34.7 15.9 %gather_fusion = bf16[3072,2048]{1,0:T(8,128)(2,1)} fusion(bf16[192,2048]{1,0:T(8,128)(2,1)S(1)} %fusion.11, s32[3072]{0:T(1024)S(1)} %broadcast_clamp_fusion), kind=kCustom, calls=%fused_computation | custom fusion | bytes 25178112 | tf_op jit(solution)/shard_map/gather | solution.py:121
  50.7 3.0 constant_dynamic-slice_fusion
  53.7 2.8 copy.64
  56.5 11.3 %all-to-all-start.6 = ((bf16[32,2,6,2048]{3,1,2,0:T(2,128)(2,1)}), bf16[32,2,6,2048]{3,1,2,0:T(2,128)(2,1)S(1)}, u32[]{:S(2)}, u32[]{:S(2)}) async-start(bf16[32,2,6,2048]{3,1,2,0:T(2,128)(2,1)} %copy.64), calls=%async_computation.6 | async-start | bytes 3145728 | tf_op jit(solution)/shard_map/all_to_all | solution.py:124
  68.7 38.4 %all-to-all-done.6 = bf16[32,2,6,2048]{3,1,2,0:T(2,128)(2,1)S(1)} async-done(((bf16[32,2,6,2048]{3,1,2,0:T(2,128)(2,1)}), bf16[32,2,6,2048]{3,1,2,0:T(2,128)(2,1)S(1)}, u32[]{:S(2)}, u32[]{:S(2)}) %all-to-all-start.6) | async-done | bytes 1572896 | tf_op jit(solution)/shard_map/all_to_all | solution.py:124
  112.9 23.9 %all_to_all.57 = bf16[32,1,2,32,128]{4,3,2,1,0:T(8,128)(2,1)S(1)} all-to-all(bf16[32,1,2,32,128]{4,3,2,1,0:T(8,128)(2,1)S(1)} %get-tuple-element.13), channel_id=1, replica_groups=mesh['fs'=32,'tp'=8] {'fs'}, dimensions={0} | all-to-all | bytes 1048576 | tf_op jit(solution)/shard_map/all_to_all | solution.py:34
  136.8 5.0 %all-to-all-start.1 = ((bf16[32,1,2,32,128]{4,3,2,1,0:T(8,128)(2,1)}), bf16[32,1,2,32,128]{4,3,2,1,0:T(8,128)(2,1)S(1)}, u32[]{:S(2)}, u32[]{:S(2)}) async-start(bf16[32,1,2,32,128]{4,3,2,1,0:T(8,128)(2,1)} %get-tuple-element.14), calls=%async_computation.1 | async-start | bytes 1048576 | tf_op jit(solution)/shard_map/all_to_all | solution.py:34
  142.8 15.6 %all-to-all-done.1 = bf16[32,1,2,32,128]{4,3,2,1,0:T(8,128)(2,1)S(1)} async-done(((bf16[32,1,2,32,128]{4,3,2,1,0:T(8,128)(2,1)}), bf16[32,1,2,32,128]{4,3,2,1,0:T(8,128)(2,1)S(1)}, u32[]{:S(2)}, u32[]{:S(2)}) %all-to-all-start.1) | async-done | bytes 524320 | tf_op jit(solution)/shard_map/all_to_all | solution.py:34
  158.4 21.5 %all_to_all.58 = bf16[32,1,2,32,128]{4,3,2,1,0:T(8,128)(2,1)S(1)} all-to-all(bf16[32,1,2,32,128]{4,3,2,1,0:T(8,128)(2,1)S(1)} %get-tuple-element.11), channel_id=1, replica_groups=mesh['fs'=32,'tp'=8] {'fs'}, dimensions={0} | all-to-all | bytes 1048576 | tf_op jit(solution)/shard_map/all_to_all | solution.py:34
  179.9 5.1 %all-to-all-start.3 = ((bf16[32,1,2,32,128]{4,3,2,1,0:T(8,128)(2,1)}), bf16[32,1,2,32,128]{4,3,2,1,0:T(8,128)(2,1)S(1)}, u32[]{:S(2)}, u32[]{:S(2)}) async-start(bf16[32,1,2,32,128]{4,3,2,1,0:T(8,128)(2,1)} %get-tuple-element.12), calls=%async_computation.3 | async-start | bytes 1048576 | tf_op jit(solution)/shard_map/all_to_all | solution.py:34
  185.5 16.0 %all-to-all-done.3 = bf16[32,1,2,32,128]{4,3,2,1,0:T(8,128)(2,1)S(1)} async-done(((bf16[32,1,2,32,128]{4,3,2,1,0:T(8,128)(2,1)}), bf16[32,1,2,32,128]{4,3,2,1,0:T(8,128)(2,1)S(1)}, u32[]{:S(2)}, u32[]{:S(2)}) %all-to-all-start.3) | async-done | bytes 524320 | tf_op jit(solution)/shard_map/all_to_all | solution.py:34
  204.5 18.0 %all-gather.6.cloned.1.call-done = bf16[32,2,48,2048]{3,0,1,2:T(8,128)(2,1)} async-done(((bf16[32,2,6,2048]{3,0,1,2:T(8,128)(2,1)}), bf16[32,2,48,2048]{3,0,1,2:T(8,128)(2,1)}) %all-gather.6.cloned.1.call-update) | async-done | bytes 12582928 | tf_op jit(solution)/shard_map/all_gather | solution.py:125
  222.5 18.0 %fusion.2 = f32[2,128,32,48]{1,3,2,0:T(8,128)S(1)} fusion(bf16[2,2048,128,1]{2,1,3,0:T(8,128)(2,1)S(1)} %bitcast.108, bf16[32,2,48,2048]{3,0,1,2:T(8,128)(2,1)} %all-gather.6.cloned.1.call-done), kind=kOutput, calls=%fused_computation.5 | convolution fusion | flops 1610612736 | bytes 15204352 | tf_op jit(solution)/shard_map/secn,enf->secf/dot_general | solution.py:62
  240.6 13.8 %fusion.13 = bf16[128,32,2,48]{0,3,1,2:T(8,128)(2,1)S(1)} fusion(f32[2,128,32,48]{1,3,2,0:T(8,128)S(1)} %fusion.2, bf16[2,2048,128,1]{2,1,3,0:T(8,128)(2,1)S(1)} %bitcast.110, bf16[32,2,48,2048]{3,0,1,2:T(8,128)(2,1)} %all-gather.6.cloned.1.call-done), kind=kOutput, calls=%fused_computation.20 | convolution fusion | flops 1612972032 | bytes 15990784 | tf_op jit(solution)/shard_map/secn,enf->secf/dot_general | solution.py:63
  257.4 10.1 %all-to-all-start.4 = ((bf16[32,2,32,256]{3,2,1,0:T(8,128)(2,1)}), bf16[32,2,32,256]{3,2,1,0:T(8,128)(2,1)S(1)}, u32[]{:S(2)}, u32[]{:S(2)}) async-start(bf16[32,2,32,256]{3,2,1,0:T(8,128)(2,1)} %bitcast.6), calls=%async_computation.4 | async-start | bytes 2097152 | tf_op jit(solution)/shard_map/all_to_all | solution.py:129
  286.9 8.2 %all-to-all-done.4 = bf16[32,2,32,256]{3,2,1,0:T(8,128)(2,1)S(1)} async-done(((bf16[32,2,32,256]{3,2,1,0:T(8,128)(2,1)}), bf16[32,2,32,256]{3,2,1,0:T(8,128)(2,1)S(1)}, u32[]{:S(2)}, u32[]{:S(2)}) %all-to-all-start.4) | async-done | bytes 1048608 | tf_op jit(solution)/shard_map/all_to_all | solution.py:129
  295.0 6.5 %all-to-all-start.5 = ((bf16[32,32,256]{2,1,0:T(8,128)(2,1)}), bf16[32,32,256]{2,1,0:T(8,128)(2,1)S(1)}, u32[]{:S(2)}, u32[]{:S(2)}) async-start(bf16[32,32,256]{2,1,0:T(8,128)(2,1)} %bitcast.10), calls=%async_computation.5 | async-start | bytes 1048576 | tf_op jit(solution)/shard_map/all_to_all | solution.py:106
  301.6 3.0 all-gather.8.cloned.1.call-done
  310.6 7.2 %all-to-all-done.5 = bf16[32,32,256]{2,1,0:T(8,128)(2,1)S(1)} async-done(((bf16[32,32,256]{2,1,0:T(8,128)(2,1)}), bf16[32,32,256]{2,1,0:T(8,128)(2,1)S(1)}, u32[]{:S(2)}, u32[]{:S(2)}) %all-to-all-start.5) | async-done | bytes 524320 | tf_op jit(solution)/shard_map/all_to_all | solution.py:106
  317.8 5.1 %all-to-all-start.7 = ((bf16[32,2,48,256]{3,2,1,0:T(8,128)(2,1)}), bf16[32,2,48,256]{3,2,1,0:T(8,128)(2,1)S(1)}, u32[]{:S(2)}, u32[]{:S(2)}) async-start(bf16[32,2,48,256]{3,2,1,0:T(8,128)(2,1)} %copy.70), calls=%async_computation.7 | async-start | bytes 3145728 | tf_op jit(solution)/shard_map/all_to_all | solution.py:139
  323.1 37.2 %all-to-all-done.7 = bf16[32,2,48,256]{3,2,1,0:T(8,128)(2,1)S(1)} async-done(((bf16[32,2,48,256]{3,2,1,0:T(8,128)(2,1)}), bf16[32,2,48,256]{3,2,1,0:T(8,128)(2,1)S(1)}, u32[]{:S(2)}, u32[]{:S(2)}) %all-to-all-start.7) | async-done | bytes 1572896 | tf_op jit(solution)/shard_map/all_to_all | solution.py:139
  360.3 4.8 %gather_fusion.1 = bf16[1536,256]{1,0:T(8,128)(2,1)S(1)} fusion(bf16[3072,256]{1,0:T(8,128)(2,1)S(1)} %bitcast.98, s32[2048]{0:T(1024)S(1)} %pad_clamp_fusion), kind=kCustom, calls=%fused_computation.1 | custom fusion | bytes 1579008 | tf_op jit(solution)/shard_map/gather | solution.py:144
  (117 shorter events, 45.9 us)
Async XLA Ops:
  8.3 19.2 %copy-start.13 = (s32[2]{0:T(128)S(1)}, s32[2]{0:T(128)}, u32[]{:S(2)}) copy-start(s32[2]{0:T(128)} %constant.57) | copy-start | bytes 28
  8.4 19.3 %copy-start.12 = (s32[2]{0:T(128)S(1)}, s32[2]{0:T(128)}, u32[]{:S(2)}) copy-start(s32[2]{0:T(128)} %constant.60) | copy-start | bytes 28
  8.4 25.9 %copy-start = (bf16[192,2048]{1,0:T(8,128)(2,1)S(1)}, bf16[192,2048]{1,0:T(8,128)(2,1)}, u32[]{:S(2)}) copy-start(bf16[192,2048]{1,0:T(8,128)(2,1)} %param.10) | copy-start | bytes 2359300
  56.5 11.4 %copy-start.7 = (f32[64,128]{1,0:T(8,128)S(1)}, f32[64,128]{1,0:T(8,128)}, u32[]{:S(2)}) copy-start(f32[64,128]{1,0:T(8,128)} %param.15) | copy-start | bytes 98308
  56.5 11.4 %copy-start.8 = (f32[64,128]{1,0:T(8,128)S(1)}, f32[64,128]{1,0:T(8,128)}, u32[]{:S(2)}) copy-start(f32[64,128]{1,0:T(8,128)} %param.16) | copy-start | bytes 98308
  56.5 11.4 %copy-start.11 = (f32[64]{0:T(128)S(1)}, f32[64]{0:T(128)}, u32[]{:S(2)}) copy-start(f32[64]{0:T(128)} %param.11) | copy-start | bytes 772
  56.5 50.6 %all-to-all-start.6 = ((bf16[32,2,6,2048]{3,1,2,0:T(2,128)(2,1)}), bf16[32,2,6,2048]{3,1,2,0:T(2,128)(2,1)S(1)}, u32[]{:S(2)}, u32[]{:S(2)}) async-start(bf16[32,2,6,2048]{3,1,2,0:T(2,128)(2,1)} %copy.64), calls=%async_computation.6 | async-start | bytes 3145728 | tf_op jit(solution)/shard_map/all_to_all | solution.py:124
  67.8 133.9 %all-gather.4.cloned.1.call-start = ((), (), s32[]{:S(2)}) async-start(), calls=%async_computation.8 | async-start | bytes 1081344 | tf_op jit(solution)/shard_map/all_gather | solution.py:44
  68.6 153.9 %all-gather.6.cloned.1.call-start = ((), (), s32[]{:S(2)}) async-start(), calls=%async_computation.9 | async-start | bytes 14155776 | tf_op jit(solution)/shard_map/all_gather | solution.py:125
  136.8 21.6 %all-to-all-start.1 = ((bf16[32,1,2,32,128]{4,3,2,1,0:T(8,128)(2,1)}), bf16[32,1,2,32,128]{4,3,2,1,0:T(8,128)(2,1)S(1)}, u32[]{:S(2)}, u32[]{:S(2)}) async-start(bf16[32,1,2,32,128]{4,3,2,1,0:T(8,128)(2,1)} %get-tuple-element.14), calls=%async_computation.1 | async-start | bytes 1048576 | tf_op jit(solution)/shard_map/all_to_all | solution.py:34
  179.9 21.5 %all-to-all-start.3 = ((bf16[32,1,2,32,128]{4,3,2,1,0:T(8,128)(2,1)}), bf16[32,1,2,32,128]{4,3,2,1,0:T(8,128)(2,1)S(1)}, u32[]{:S(2)}, u32[]{:S(2)}) async-start(bf16[32,1,2,32,128]{4,3,2,1,0:T(8,128)(2,1)} %get-tuple-element.12), calls=%async_computation.3 | async-start | bytes 1048576 | tf_op jit(solution)/shard_map/all_to_all | solution.py:34
  185.0 119.6 %all-gather.8.cloned.1.call-start = ((), (), s32[]{:S(2)}) async-start(), calls=%async_computation.10 | async-start | bytes 7520256 | tf_op jit(solution)/shard_map/all_gather | solution.py:51
  185.5 37.0 %copy-start.3 = (bf16[1,2,32,64,128]{4,3,2,1,0:T(8,128)(2,1)}, bf16[1,2,32,64,128]{4,3,2,1,0:T(8,128)(2,1)S(1)}, u32[]{:S(2)}) copy-start(bf16[1,2,32,64,128]{4,3,2,1,0:T(8,128)(2,1)S(1)} %copy.55) | copy-start | bytes 3145732
  201.6 38.9 %copy-start.4 = (bf16[1,2,32,64,128]{4,3,2,1,0:T(8,128)(2,1)}, bf16[1,2,32,64,128]{4,3,2,1,0:T(8,128)(2,1)S(1)}, u32[]{:S(2)}) copy-start(bf16[1,2,32,64,128]{4,3,2,1,0:T(8,128)(2,1)S(1)} %copy.56) | copy-start | bytes 3145732
  203.3 0.8 copy-start.6
  203.3 37.2 %copy-start.2 = (bf16[2048,128]{1,0:T(8,128)(2,1)}, bf16[2048,128]{1,0:T(8,128)(2,1)S(1)}, u32[]{:S(2)}) copy-start(bf16[2048,128]{1,0:T(8,128)(2,1)S(1)} %get-tuple-element.36) | copy-start | bytes 1572868
  254.3 1.9 copy-start.1
  256.2 11.2 %copy-start.9 = (f32[32,256]{1,0:T(8,128)S(1)}, f32[32,256]{1,0:T(8,128)}, u32[]{:S(2)}) copy-start(f32[32,256]{1,0:T(8,128)} %param.17) | copy-start | bytes 98308
  257.4 37.7 %all-to-all-start.4 = ((bf16[32,2,32,256]{3,2,1,0:T(8,128)(2,1)}), bf16[32,2,32,256]{3,2,1,0:T(8,128)(2,1)S(1)}, u32[]{:S(2)}, u32[]{:S(2)}) async-start(bf16[32,2,32,256]{3,2,1,0:T(8,128)(2,1)} %bitcast.6), calls=%async_computation.4 | async-start | bytes 2097152 | tf_op jit(solution)/shard_map/all_to_all | solution.py:129
  295.0 22.8 %all-to-all-start.5 = ((bf16[32,32,256]{2,1,0:T(8,128)(2,1)}), bf16[32,32,256]{2,1,0:T(8,128)(2,1)S(1)}, u32[]{:S(2)}, u32[]{:S(2)}) async-start(bf16[32,32,256]{2,1,0:T(8,128)(2,1)} %bitcast.10), calls=%async_computation.5 | async-start | bytes 1048576 | tf_op jit(solution)/shard_map/all_to_all | solution.py:106
  301.6 3.0 copy-start.5
  304.6 2.8 slice-start
  310.6 12.3 %copy-start.10 = (f32[192,8]{0,1:T(8,128)S(1)}, f32[192,8]{0,1:T(8,128)}, u32[]{:S(2)}) copy-start(f32[192,8]{0,1:T(8,128)} %param.19) | copy-start | bytes 18436
  317.8 42.5 %all-to-all-start.7 = ((bf16[32,2,48,256]{3,2,1,0:T(8,128)(2,1)}), bf16[32,2,48,256]{3,2,1,0:T(8,128)(2,1)S(1)}, u32[]{:S(2)}, u32[]{:S(2)}) async-start(bf16[32,2,48,256]{3,2,1,0:T(8,128)(2,1)} %copy.70), calls=%async_computation.7 | async-start | bytes 3145728 | tf_op jit(solution)/shard_map/all_to_all | solution.py:139
Sparse Core Ops, SparseCore 0:
  71.8 80.5 all-gather.3
  154.2 68.2 all-gather.5
  255.5 49.0 all-gather.7
